TPU v7x, 32 devices: a whole 2x2x4 slice. The times are simulated.
32 devices in a mesh: grp: 2 (over y), ep: 4 (over z), tp: 4 (over x, core).
Axes of the slice: x: 2, y: 2, z: 4, core: 2. Of those that a mesh axis runs over, the one named last changes fastest.
Arguments:
- queries: bfloat16 [4096, 768], P(('grp', 'ep'), 'tp'), parts along dimension 0, may hold values from -6 to 6
- key_value: bfloat16 [4096, 4, 128], P(('grp', 'ep'), 'tp'), parts along dimension 0, may hold values from -6 to 6
- key_bias: bfloat16 [4, 4096], P('tp', ('grp', 'ep')), parts along dimension 1, may hold values from -20 to 0
- out_weight: bfloat16 [768, 2048], P('tp'), may hold values from -0.75 to 0.75
- expert_input: bfloat16 [4096, 2048], P(('grp', 'ep', 'tp')), parts along dimension 0, may hold values from -6 to 6
- norm_gain: float32 [2048], replicated, may hold values from 0.1 to 1.9
- routes: int32 [4096, 4], P(('grp', 'ep', 'tp')), parts along dimension 0, may hold values from 0 to 15, as said below
- route_weights: float32 [4096, 4], P(('grp', 'ep', 'tp')), parts along dimension 0, may hold values from 0.2 to 1
- gate_weight: bfloat16 [16, 2048, 512], P(('ep', 'tp')), may hold values from -0.125 to 0.125
- up_weight: bfloat16 [16, 2048, 512], P(('ep', 'tp')), may hold values from -0.125 to 0.125
- down_weight: bfloat16 [16, 512, 2048], P(('ep', 'tp')), may hold values from -0.25 to 0.25
- shared_gate: bfloat16 [2048, 256], replicated, may hold values from -0.125 to 0.125
- shared_up: bfloat16 [2048, 256], replicated, may hold values from -0.125 to 0.125
- shared_down: bfloat16 [256, 2048], replicated, may hold values from -0.375 to 0.375
Outputs:
- mixer_output: bfloat16 [4096, 2048], P(('grp', 'ep', 'tp')), parts along dimension 0
- expert_output: bfloat16 [4096, 2048], P(('grp', 'ep', 'tp')), parts along dimension 0
There are 2 independent parts, one for each index of `grp`. A program takes and returns all parts, laid end to end along the dimension named above; an argument that names none is the same for every part. Nothing has to cross between parts.
Inputs may be any that keep to these rules, and one draw needn't show every extreme that they name: `routes`: each row names 4 different experts. Among the 128 rows of one device no expert is named more than 48 times, and in every draw one expert is named exactly 48 times in the rows of every device.
All inputs are finite; a program needn't handle non-finite values.
Results may differ from a plain program's by a relative error of at most 0.009.
Values may be sent and summed in bfloat16 or wider, within the bound.
A program may use at most 128 MiB of HBM per device.

v0:
```python
import jax
import jax.numpy as jnp
from jax import lax
from jax.sharding import PartitionSpec as P


def passed_along(block, axis, distance):
    devices = range(lax.axis_size(axis))
    route = [(i - distance, i) for i in devices if i - distance in devices]
    return lax.ppermute(block, axis, route)


def piece_update(running, query_rows, key_rows, value_rows, key_offset, allowed):
    totals, kept_sum = running
    logits = (
        jnp.einsum("sgrd,kgd->grsk", query_rows, key_rows, preferred_element_type=jnp.float32)
        * 0.125
    )
    logits = logits + key_offset.astype(jnp.float32)[:, None, None, :]
    log_keep = jnp.where(allowed, -jax.nn.softplus(logits), 0.0)
    log_after = lax.cumsum(log_keep, axis=3, reverse=True) - log_keep
    weights = jnp.where(
        allowed, jnp.exp(jax.nn.log_sigmoid(logits) + log_after + kept_sum[..., None]), 0.0
    )
    weights = weights.astype(jnp.bfloat16)
    totals = totals + jnp.einsum(
        "grsk,kgd->grsd", weights, value_rows, preferred_element_type=jnp.float32
    )
    return (totals, kept_sum + jnp.sum(log_keep, axis=3))


def mixer_half(queries, key_value, key_bias, out_weight):
    span_rows, key_groups, pair_width = key_value.shape
    head_dim = pair_width // 2
    per_group = queries.shape[1] // (key_groups * head_dim)
    query_rows = queries.reshape(span_rows, key_groups, per_group, head_dim)
    axis_size = lax.axis_size("ep")
    chain_length = axis_size // max(1, axis_size // 4)
    device_place = lax.axis_index("ep")
    chain_place = jnp.minimum((device_place + 2) % chain_length, device_place)
    positions = jnp.arange(span_rows, dtype=jnp.int32)
    strict_mask = positions[None, :] < positions[:, None]
    full_mask = jnp.ones((span_rows, span_rows), dtype=bool)
    initial = (
        jnp.zeros((key_groups, per_group, span_rows, head_dim), jnp.float32),
        jnp.zeros((key_groups, per_group, span_rows), jnp.float32),
    )
    running = piece_update(
        initial,
        query_rows,
        key_value[..., :head_dim],
        key_value[..., head_dim:],
        key_bias,
        strict_mask,
    )

    def advance(distance, loop_state):
        current, visiting_keys, visiting_bias = loop_state
        visiting_keys, visiting_bias = passed_along((visiting_keys, visiting_bias), "ep", 1)

        def include(earlier_state):
            return piece_update(
                earlier_state,
                query_rows,
                visiting_keys[..., :head_dim],
                visiting_keys[..., head_dim:],
                visiting_bias,
                full_mask,
            )

        def skip(earlier_state):
            return earlier_state

        current = lax.cond(distance <= chain_place, include, skip, current)
        return (current, visiting_keys, visiting_bias)

    running, _, _ = lax.fori_loop(1, chain_length, advance, (running, key_value, key_bias))
    attended = running[0].astype(jnp.bfloat16)
    projection = out_weight.reshape(key_groups, per_group, head_dim, out_weight.shape[1])
    return lax.psum_scatter(
        jnp.einsum(
            "grsd,grde->se", attended, projection, preferred_element_type=jnp.float32
        ).astype(jnp.bfloat16),
        "tp",
        scatter_dimension=0,
        tiled=True,
    )


def expert_rows(arrived, gate_weight, up_weight, down_weight):
    sources, capacity, model_width = arrived.shape
    flat_rows = arrived.reshape(sources * capacity, model_width)
    gate_part = jnp.dot(flat_rows, gate_weight[0], preferred_element_type=jnp.float32)
    up_part = jnp.dot(flat_rows, up_weight[0], preferred_element_type=jnp.float32)
    hidden = (jax.nn.silu(gate_part) * up_part).astype(jnp.bfloat16)
    result = jnp.dot(hidden, down_weight[0], preferred_element_type=jnp.float32).astype(
        jnp.bfloat16
    )
    return result.reshape(sources, capacity, model_width)


def experts_half(
    expert_input,
    norm_gain,
    routes,
    route_weights,
    gate_weight,
    up_weight,
    down_weight,
    shared_gate,
    shared_up,
    shared_down,
):
    tokens, top_count = routes.shape
    model_width = expert_input.shape[1]
    ep_count = lax.axis_size("ep")
    tp_count = lax.axis_size("tp")
    experts = ep_count * tp_count
    capacity = max(2, 3 * tokens * top_count // (2 * experts))
    widened = expert_input.astype(jnp.float32)
    normed = (
        widened * lax.rsqrt(jnp.mean(widened * widened, axis=-1, keepdims=True) + 1e-06) * norm_gain
    ).astype(jnp.bfloat16)
    flat_routes = routes.reshape(-1)
    one_hot = (flat_routes[:, None] == jnp.arange(experts, dtype=jnp.int32)[None, :]).astype(
        jnp.int32
    )
    before = jnp.cumsum(one_hot, axis=0) - one_hot
    slot_index = jnp.sum(before * one_hot, axis=1)
    target = flat_routes * capacity + slot_index
    picker = (jnp.arange(experts * capacity, dtype=jnp.int32)[:, None] == target[None, :]).astype(
        jnp.bfloat16
    )
    picker = jnp.sum(picker.reshape(experts * capacity, tokens, top_count), axis=2)
    outgoing = jnp.dot(picker, normed, preferred_element_type=jnp.float32).astype(jnp.bfloat16)
    outgoing = outgoing.reshape(experts, capacity, model_width)
    came_back = lax.all_to_all(
        expert_rows(
            lax.all_to_all(outgoing, ("ep", "tp"), split_axis=0, concat_axis=0, tiled=True),
            gate_weight,
            up_weight,
            down_weight,
        ),
        ("ep", "tp"),
        split_axis=0,
        concat_axis=0,
        tiled=True,
    )
    back_rows = came_back.reshape(experts * capacity, model_width)
    picked = jnp.take(back_rows, target, axis=0).reshape(tokens, top_count, model_width)
    routed = jnp.sum(picked.astype(jnp.float32) * route_weights[:, :, None], axis=1)
    shared_hidden = (
        jax.nn.silu(jnp.dot(normed, shared_gate, preferred_element_type=jnp.float32))
        * jnp.dot(normed, shared_up, preferred_element_type=jnp.float32)
    ).astype(jnp.bfloat16)
    shared_term = jnp.dot(shared_hidden, shared_down, preferred_element_type=jnp.float32)
    return (routed + shared_term).astype(jnp.bfloat16)


def per_device(
    queries,
    key_value,
    key_bias,
    out_weight,
    expert_input,
    norm_gain,
    routes,
    route_weights,
    gate_weight,
    up_weight,
    down_weight,
    shared_gate,
    shared_up,
    shared_down,
):
    mixer_output = mixer_half(queries, key_value, key_bias, out_weight)
    expert_output = experts_half(
        expert_input,
        norm_gain,
        routes,
        route_weights,
        gate_weight,
        up_weight,
        down_weight,
        shared_gate,
        shared_up,
        shared_down,
    )
    return (mixer_output, expert_output)


def solution(mesh):
    placed = (
        P(("grp", "ep"), "tp"),
        P(("grp", "ep"), "tp", None),
        P("tp", ("grp", "ep")),
        P("tp", None),
        P(("grp", "ep", "tp"), None),
        P(),
        P(("grp", "ep", "tp"), None),
        P(("grp", "ep", "tp"), None),
        P(("ep", "tp"), None, None),
        P(("ep", "tp"), None, None),
        P(("ep", "tp"), None, None),
        P(),
        P(),
        P(),
    )
    return jax.shard_map(
        per_device,
        mesh=mesh,
        in_specs=placed,
        out_specs=(P(("grp", "ep", "tp"), None), P(("grp", "ep", "tp"), None)),
        check_vma=False,
    )
```

profile of v0, /device:TPU:0, one launch (start us, length us, event | category | flops | bytes accessed | tf_op | source)
XLA Modules:
  0.0 265.7 jit_solution(3107453401127544733)
XLA Ops:
  7.2 0.0 copy-start
  7.2 0.8 copy.101
  8.0 0.8 copy.66
  8.8 0.1 eq.42
  8.9 0.1 reshape.253
  9.0 1.2 reduce-window.26
  10.2 0.2 slice_reduce_fusion
  10.4 0.1 fusion.74
  10.5 0.1 reduce_sum.66
  10.7 0.1 copy.69
  10.7 0.7 compare_and_fusion
  11.4 0.2 fusion.60
  11.6 1.2 fusion.57
  12.8 2.1 convolution_convert_fusion.1
  15.0 0.0 copy-start.7
  15.0 76.9 %all_to_all.10 = bf16[16,48,2048]{2,1,0:T(8,128)(2,1)S(1)} all-to-all(bf16[16,48,2048]{2,1,0:T(8,128)(2,1)S(1)} %bitcast.200), channel_id=1, replica_groups=mesh['grp'=2,'ep'=4,'tp'=4] {'ep','tp'}, dimensions={0} | all-to-all | bytes 6291456 | tf_op jit(solution)/shard_map/all_to_all | solution.py:139
  91.9 1.7 copy-done.2
  93.6 0.0 copy-done.7
  93.6 2.9 %fusion.46 = f32[768,512]{1,0:T(8,128)} fusion(bf16[768,2048]{1,0:T(8,128)(2,1)S(1)} %bitcast.203, bf16[1,2048,512]{2,1,0:T(8,128)(2,1)S(1)} %copy-done.7), kind=kOutput, calls=%fused_computation.65 | convolution fusion | flops 1610612736 | bytes 6815744 | tf_op jit(solution)/shard_map/dot_general | solution.py:93
  96.6 0.0 copy-done
  96.6 8.1 %convolution_convert_fusion = bf16[768,2048]{1,0:T(8,128)(2,1)} fusion(bf16[1,512,2048]{2,1,0:T(8,128)(2,1)S(1)} %copy-done, f32[768,512]{1,0:T(8,128)} %fusion.46, bf16[768,2048]{1,0:T(8,128)(2,1)} %bitcast.204, bf16[1,2048,512]{2,1,0:T(8,128)(2,1)} %param.27), kind=kOutput, calls=%fused_computation.39 | convolution fusion | flops 3225157632 | bytes 12058624 | tf_op jit(solution)/shard_map/dot_general | solution.py:96
  104.7 5.4 %all-to-all-start.1 = ((bf16[16,48,2048]{2,1,0:T(8,128)(2,1)}), bf16[16,48,2048]{2,1,0:T(8,128)(2,1)}, u32[]{:S(2)}, u32[]{:S(2)}) async-start(bf16[16,48,2048]{2,1,0:T(8,128)(2,1)} %bitcast.201), calls=%async_computation.2 | async-start | bytes 6291456 | tf_op jit(solution)/shard_map/all_to_all | solution.py:137
  110.1 0.2 reduce-scatter.2.cloned.1.call-start
  110.4 0.0 copy-done.3
  110.4 0.1 copy.60
  110.5 0.1 iota_compare_fusion.1
  110.6 0.0 copy-done.8
  110.6 4.1 %fusion.79 = (f32[3,512]{1,0:T(4,128)S(1)}, f32[1,3,512,512]{2,3,1,0:T(8,128)S(1)}, f32[512,512,3]{1,0,2:T(8,128)}) fusion(f32[512]{0:T(512)S(1)} %bitcast.211, pred[512,512]{0,1:T(8,128)(4,1)S(1)} %iota_compare_fusion.1, bf16[512,3,64]{0,2,1:T(8,128)(2,1)S(1)} %bitcast.214, bf16[512,1,128]{0,2,1:T(8,128)(2,1)S(1)} %copy.60), kind=kOutput, calls=%fused_computation.113 | convolution fusion | flops 109312512 | bytes 6823936 | tf_op jit(solution)/shard_map/sgrd,kgd->grsk/dot_general | solution.py:16
  114.7 14.9 %fusion.40 = f32[1,3,512,4,128]{2,3,4,1,0:T(4,128)S(1)} fusion(f32[1,3,512,4,128]{2,4,3,1,0:T(8,128)S(1)} %bitcast.202), kind=kOutput, calls=%fused_computation.58 | output fusion | flops 99876864 | bytes 6291456 | tf_op jit(solution)/shard_map/reduce-window.2
  129.6 2.6 copy.62
  132.2 0.1 reduce-window.23
  132.3 6.8 %fusion.32 = bf16[1,3,512,512]{2,3,1,0:T(8,128)(2,1)S(1)} fusion(f32[1,3,512,4,128]{2,4,3,1,0:T(8,128)} %copy.62, f32[512,512,3]{1,0,2:T(8,128)} %get-tuple-element.201, f32[3,512,4]{1,2,0:T(4,128)S(1)} %slice_bitcast_fusion.6, f32[512]{0:T(512)S(1)} %bitcast.212, pred[512,512]{0,1:T(8,128)(4,1)S(1)} %iota_compare_fusion.1), kind=kLoop, calls=%fused_computation.45 | loop fusion | flops 18087936 | bytes 8153088 | tf_op jit(solution)/shard_map/convert_element_type | solution.py:25
  139.1 0.4 fusion.53
  139.5 84.5 %while.19 = (s32[]{:T(128)}, f32[1,3,512,64]{2,3,1,0:T(8,128)S(1)}, f32[1,3,512]{2,1,0:T(4,128)S(1)}, bf16[512,1,128]{0,2,1:T(8,128)(2,1)S(1)}, bf16[1,512]{1,0:...) while((s32[]{:T(128)}, f32[1,3,512,64]{2,3,1,0:T(8,128)S(1)}, ...), condition=%wide.region_9.10_spmd, body=%wide.region_3.0_spmd.sunk | while | flops 326492672 | bytes 30434568 | solution.py:77
  139.7 3.8 %collective-permute-start = (bf16[512,1,128]{0,2,1:T(8,128)(2,1)S(1)}, bf16[512,1,128]{0,2,1:T(8,128)(2,1)S(1)}, u32[]{:S(2)}, u32[]{:S(2)}) collective-permute-start(bf16[512,1,128]{0,2,1:T(8,128)(2,1)S(1)} %get-tuple-element.264), channel_id=1, source_target_pairs={{0,4},{4,8},{8,12},{1,5},{5,9},{9,13},{2,6},{6,10},{10,14},{3,7},{... | collective-permute-start | bytes 393224 | tf_op jit(solution)/shard_map/while/body/eval_jaxpr/ppermute | solution.py:10
  143.5 3.4 %collective-permute-start.1 = (bf16[1,512]{1,0:T(2,128)(2,1)S(1)}, bf16[1,512]{1,0:T(2,128)(2,1)S(1)}, u32[]{:S(2)}, u32[]{:S(2)}) collective-permute-start(bf16[1,512]{1,0:T(2,128)(2,1)S(1)} %get-tuple-element.265), channel_id=1, source_target_pairs={{0,4},{4,8},{8,12},{1,5},{5,9},{9,13},{2,6},{6,10},{10,14},{3,7},{... | collective-permute-start | bytes 3080 | tf_op jit(solution)/shard_map/while/body/eval_jaxpr/ppermute | solution.py:10
  146.8 17.8 %collective-permute-done.1 = bf16[1,512]{1,0:T(2,128)(2,1)S(1)} collective-permute-done((bf16[1,512]{1,0:T(2,128)(2,1)S(1)}, bf16[1,512]{1,0:T(2,128)(2,1)S(1)}, u32[]{:S(2)}, u32[]{:S(2)}) %collective-permute-start.1) | collective-permute-done | bytes 1056 | tf_op jit(solution)/shard_map/while/body/eval_jaxpr/ppermute | solution.py:10
  164.7 0.0 collective-permute-done
  164.7 48.4 %collective-permute-start = (bf16[512,1,128]{0,2,1:T(8,128)(2,1)S(1)}, bf16[512,1,128]{0,2,1:T(8,128)(2,1)S(1)}, u32[]{:S(2)}, u32[]{:S(2)}) collective-permute-start(bf16[512,1,128]{0,2,1:T(8,128)(2,1)S(1)} %get-tuple-element.264), channel_id=1, source_target_pairs={{0,4},{4,8},{8,12},{1,5},{5,9},{9,13},{2,6},{6,10},{10,14},{3,7},{... | collective-permute-start | bytes 393224 | tf_op jit(solution)/shard_map/while/body/eval_jaxpr/ppermute | solution.py:10
  213.1 1.9 collective-permute-start.1
  215.0 1.3 collective-permute-done.1
  216.3 0.0 collective-permute-done
  216.4 4.2 %collective-permute-start = (bf16[512,1,128]{0,2,1:T(8,128)(2,1)S(1)}, bf16[512,1,128]{0,2,1:T(8,128)(2,1)S(1)}, u32[]{:S(2)}, u32[]{:S(2)}) collective-permute-start(bf16[512,1,128]{0,2,1:T(8,128)(2,1)S(1)} %get-tuple-element.264), channel_id=1, source_target_pairs={{0,4},{4,8},{8,12},{1,5},{5,9},{9,13},{2,6},{6,10},{10,14},{3,7},{... | collective-permute-start | bytes 393224 | tf_op jit(solution)/shard_map/while/body/eval_jaxpr/ppermute | solution.py:10
  220.6 1.9 collective-permute-start.1
  222.5 1.3 collective-permute-done.1
  223.8 0.0 collective-permute-done
  224.0 0.0 copy-start.5
  224.0 0.0 copy-start.6
  224.1 0.0 copy-start.1
  224.1 0.0 copy-start.4
  224.1 3.3 %bitcast_convert_fusion = bf16[512,2048]{1,0:T(8,128)(2,1)} fusion(bf16[3,64,2048]{2,1,0:T(8,128)(2,1)} %bitcast.213, f32[1,3,512,64]{2,3,1,0:T(8,128)S(1)} %get-tuple-element.151), kind=kOutput, calls=%fused_computation.37 | convolution fusion | flops 403800064 | bytes 3276800 | tf_op jit(solution)/shard_map/grsd,grde->se/dot_general | solution.py:81
  227.4 0.0 reduce-scatter.2.cloned.1.call-update
  227.4 0.1 copy.71
  227.5 0.1 mul.93
  227.6 0.1 copy.70
  227.8 0.0 copy-done.6
  227.8 0.1 copy.72
  227.9 1.6 fusion.82
  229.5 0.0 all-to-all-done.1
  229.5 7.6 %gather_fusion = bf16[512,2048]{1,0:T(8,128)(2,1)} fusion(bf16[768,2048]{1,0:T(8,128)(2,1)} %bitcast.44, s32[1024]{0:T(1024)S(1)} %pad_clamp_fusion), kind=kCustom, calls=%fused_computation | custom fusion | bytes 4196352 | tf_op jit(solution)/shard_map/jit(_take)/gather | solution.py:150
  237.1 4.1 %gather.7 = bf16[128,4,2048]{2,1,0:T(4,128)(2,1)} reshape(bf16[512,2048]{1,0:T(8,128)(2,1)} %gather_fusion) | data formatting | bytes 4194304 | tf_op jit(solution)/shard_map/jit(_take)/gather | solution.py:150
  241.2 6.6 %multiply_reduce_fusion = f32[128,2048]{1,0:T(8,128)} fusion(f32[128,4]{1,0:T(8,128)S(1)} %copy.72, bf16[128,4,2048]{2,1,0:T(4,128)(2,1)} %gather.7, pred[128,4]{1,0:T(8,128)(4,1)S(1)} %copy.70), kind=kLoop, calls=%fused_computation.38 | loop fusion | flops 3932160 | bytes 3148288 | tf_op jit(solution)/shard_map/reduce_sum | solution.py:151
  247.8 3.5 %fusion.42 = bf16[128,2048]{1,0:T(8,128)(2,1)} fusion(f32[128,2048]{1,0:T(8,128)} %multiply_reduce_fusion, bf16[256,2048]{1,0:T(8,128)(2,1)} %param.31, bf16[2048,256]{1,0:T(8,128)(2,1)} %param.30, f32[128,256]{1,0:T(8,128)S(1)} %fusion.82, bf16[128,2048]{1,0:T(8,128)(2,1)S(1)} %copy-done.1, f32[2048]{0:T(1024)S(1)} %copy-done.4, f32[128]{0:T(128)S(1)} %add_rsqrt_fusion), kind=kOutput, calls=%fused_computation.61 | convolution fusion | flops 270204928 | bytes 4334080 | tf_op jit(solution)/shard_map/dot_general | solution.py:156
  251.3 7.4 %reduce-scatter.2.cloned.1.call-done = bf16[128,2048]{1,0:T(8,128)(2,1)} async-done(((bf16[512,2048]{1,0:T(8,128)(2,1)}), bf16[128,2048]{1,0:T(8,128)(2,1)}) %reduce-scatter.2.cloned.1.call-update) | async-done | bytes 524304 | tf_op jit(solution)/shard_map/reduce_scatter | solution.py:80
  (25 shorter events, 0.1 us)
Async XLA Ops:
  7.2 89.4 %copy-start = (bf16[1,512,2048]{2,1,0:T(8,128)(2,1)S(1)}, bf16[1,512,2048]{2,1,0:T(8,128)(2,1)}, u32[]{:S(2)}) copy-start(bf16[1,512,2048]{2,1,0:T(8,128)(2,1)} %param.28) | copy-start | bytes 6291460
  15.0 78.7 %copy-start.7 = (bf16[1,2048,512]{2,1,0:T(8,128)(2,1)S(1)}, bf16[1,2048,512]{2,1,0:T(8,128)(2,1)}, u32[]{:S(2)}) copy-start(bf16[1,2048,512]{2,1,0:T(8,128)(2,1)} %param.26) | copy-start | bytes 6291460
  91.9 1.7 copy-start.2
  104.7 5.6 %copy-start.3 = (bf16[512,1,128]{2,0,1:T(8,128)(2,1)S(1)}, bf16[512,1,128]{2,0,1:T(8,128)(2,1)}, u32[]{:S(2)}) copy-start(bf16[512,1,128]{2,0,1:T(8,128)(2,1)} %param.19) | copy-start | bytes 393220
  104.7 5.9 %copy-start.8 = (bf16[512,192]{0,1:T(8,128)(2,1)S(1)}, bf16[512,192]{0,1:T(8,128)(2,1)}, u32[]{:S(2)}) copy-start(bf16[512,192]{0,1:T(8,128)(2,1)} %param.18) | copy-start | bytes 589828
  104.7 124.8 %all-to-all-start.1 = ((bf16[16,48,2048]{2,1,0:T(8,128)(2,1)}), bf16[16,48,2048]{2,1,0:T(8,128)(2,1)}, u32[]{:S(2)}, u32[]{:S(2)}) async-start(bf16[16,48,2048]{2,1,0:T(8,128)(2,1)} %bitcast.201), calls=%async_computation.2 | async-start | bytes 6291456 | tf_op jit(solution)/shard_map/all_to_all | solution.py:137
  110.1 148.5 %reduce-scatter.2.cloned.1.call-start = ((), (), s32[]{:S(2)}) async-start(), calls=%async_computation.3 | async-start | bytes 2621440 | tf_op jit(solution)/shard_map/reduce_scatter | solution.py:80
  139.7 25.0 %collective-permute-start = (bf16[512,1,128]{0,2,1:T(8,128)(2,1)S(1)}, bf16[512,1,128]{0,2,1:T(8,128)(2,1)S(1)}, u32[]{:S(2)}, u32[]{:S(2)}) collective-permute-start(bf16[512,1,128]{0,2,1:T(8,128)(2,1)S(1)} %get-tuple-element.264), channel_id=1, source_target_pairs={{0,4},{4,8},{8,12},{1,5},{5,9},{9,13},{2,6},{6,10},{10,14},{3,7},{... | collective-permute-start | bytes 393224 | tf_op jit(solution)/shard_map/while/body/eval_jaxpr/ppermute | solution.py:10
  143.5 21.2 %collective-permute-start.1 = (bf16[1,512]{1,0:T(2,128)(2,1)S(1)}, bf16[1,512]{1,0:T(2,128)(2,1)S(1)}, u32[]{:S(2)}, u32[]{:S(2)}) collective-permute-start(bf16[1,512]{1,0:T(2,128)(2,1)S(1)} %get-tuple-element.265), channel_id=1, source_target_pairs={{0,4},{4,8},{8,12},{1,5},{5,9},{9,13},{2,6},{6,10},{10,14},{3,7},{... | collective-permute-start | bytes 3080 | tf_op jit(solution)/shard_map/while/body/eval_jaxpr/ppermute | solution.py:10
  164.7 51.6 %collective-permute-start = (bf16[512,1,128]{0,2,1:T(8,128)(2,1)S(1)}, bf16[512,1,128]{0,2,1:T(8,128)(2,1)S(1)}, u32[]{:S(2)}, u32[]{:S(2)}) collective-permute-start(bf16[512,1,128]{0,2,1:T(8,128)(2,1)S(1)} %get-tuple-element.264), channel_id=1, source_target_pairs={{0,4},{4,8},{8,12},{1,5},{5,9},{9,13},{2,6},{6,10},{10,14},{3,7},{... | collective-permute-start | bytes 393224 | tf_op jit(solution)/shard_map/while/body/eval_jaxpr/ppermute | solution.py:10
  213.1 3.2 %collective-permute-start.1 = (bf16[1,512]{1,0:T(2,128)(2,1)S(1)}, bf16[1,512]{1,0:T(2,128)(2,1)S(1)}, u32[]{:S(2)}, u32[]{:S(2)}) collective-permute-start(bf16[1,512]{1,0:T(2,128)(2,1)S(1)} %get-tuple-element.265), channel_id=1, source_target_pairs={{0,4},{4,8},{8,12},{1,5},{5,9},{9,13},{2,6},{6,10},{10,14},{3,7},{... | collective-permute-start | bytes 3080 | tf_op jit(solution)/shard_map/while/body/eval_jaxpr/ppermute | solution.py:10
  216.4 7.4 %collective-permute-start = (bf16[512,1,128]{0,2,1:T(8,128)(2,1)S(1)}, bf16[512,1,128]{0,2,1:T(8,128)(2,1)S(1)}, u32[]{:S(2)}, u32[]{:S(2)}) collective-permute-start(bf16[512,1,128]{0,2,1:T(8,128)(2,1)S(1)} %get-tuple-element.264), channel_id=1, source_target_pairs={{0,4},{4,8},{8,12},{1,5},{5,9},{9,13},{2,6},{6,10},{10,14},{3,7},{... | collective-permute-start | bytes 393224 | tf_op jit(solution)/shard_map/while/body/eval_jaxpr/ppermute | solution.py:10
  220.6 3.2 %collective-permute-start.1 = (bf16[1,512]{1,0:T(2,128)(2,1)S(1)}, bf16[1,512]{1,0:T(2,128)(2,1)S(1)}, u32[]{:S(2)}, u32[]{:S(2)}) collective-permute-start(bf16[1,512]{1,0:T(2,128)(2,1)S(1)} %get-tuple-element.265), channel_id=1, source_target_pairs={{0,4},{4,8},{8,12},{1,5},{5,9},{9,13},{2,6},{6,10},{10,14},{3,7},{... | collective-permute-start | bytes 3080 | tf_op jit(solution)/shard_map/while/body/eval_jaxpr/ppermute | solution.py:10
  224.0 3.4 %copy-start.5 = (s32[128,4]{0,1:T(4,128)S(1)}, s32[128,4]{0,1:T(4,128)}, u32[]{:S(2)}) copy-start(s32[128,4]{0,1:T(4,128)} %param.24) | copy-start | bytes 6148
  224.0 3.7 %copy-start.6 = (f32[128,4]{0,1:T(4,128)S(1)}, f32[128,4]{0,1:T(4,128)}, u32[]{:S(2)}) copy-start(f32[128,4]{0,1:T(4,128)} %param.25) | copy-start | bytes 6148
  224.1 3.9 %copy-start.1 = (bf16[128,2048]{1,0:T(8,128)(2,1)S(1)}, bf16[128,2048]{1,0:T(8,128)(2,1)}, u32[]{:S(2)}) copy-start(bf16[128,2048]{1,0:T(8,128)(2,1)} %param.22) | copy-start | bytes 1572868
  224.1 3.9 %copy-start.4 = (f32[2048]{0:T(1024)S(1)}, f32[2048]{0:T(1024)}, u32[]{:S(2)}) copy-start(f32[2048]{0:T(1024)} %param.23) | copy-start | bytes 24580
Sparse Core Ops, SparseCore 0:
  227.5 31.0 reduce-scatter.1
where the time goes:
time: 271 us; the launch traced here: 266 us
  blocking collectives  76.9 us (28%)
  starting transfers between devices  69.2 us (26%)
  other arithmetic  31.8 us (12%)
  waiting for transfers between devices  27.8 us (10%)
  matrix products  26 us (10%)
  local copies, waits for them, and re-layouts  18.9 us (7%)
  between operations  14.5 us (5%)
    all_to_all x1, blocking collectives, experts_half(): lax.all_to_all(outgoing, ('ep', 'tp'), split_axis=0, concat_axis=0, tiled...  76.9 us
    ppermute x6, starting transfers between devices, passed_along(): return lax.ppermute(block, axis, route)  63.6 us
    ppermute x6, waiting for transfers between devices, passed_along(): return lax.ppermute(block, axis, route)  20.4 us
    another operation x4, other arithmetic  16.1 us
    gather x2, local copies, waits for them, and re-layouts, experts_half(): jnp.take(back_rows, target, axis=0).reshape(tokens, top_count, model_width)  11.7 us
    dot_general x1, matrix products, expert_rows(): jnp.dot(hidden, down_weight[0], preferred_element_type=jnp.float32)  8.14 us
    reduce_scatter x1, waiting for transfers between devices, mixer_half(): lax.psum_scatter(jnp.einsum('grsd,grde->se', attended, projection, prefer...  7.37 us
    convert_element_type x1, other arithmetic, piece_update(): weights = weights.astype(jnp.bfloat16)  6.8 us
  transfers between devices with their start and end apart: 8, of which 4 were waited for; matrix products, arithmetic and copies ran while one was open for 21% of the time, Pallas kernels for 0%

commit v1 on v0

--- a/solution.py
+++ b/solution.py
@@ -1,7 +1,13 @@
 import jax
 import jax.numpy as jnp
 from jax import lax
+from jax.experimental import pallas as pl
+from jax.experimental.pallas import tpu as pltpu
 from jax.sharding import PartitionSpec as P
+
+MESH = pl.DeviceIdType.MESH
+F32 = jnp.float32
+BF16 = jnp.bfloat16
 
 
 def passed_along(block, axis, distance):
@@ -10,81 +16,583 @@
     return lax.ppermute(block, axis, route)
 
 
-def piece_update(running, query_rows, key_rows, value_rows, key_offset, allowed):
-    totals, kept_sum = running
-    logits = (
-        jnp.einsum("sgrd,kgd->grsk", query_rows, key_rows, preferred_element_type=jnp.float32)
-        * 0.125
-    )
-    logits = logits + key_offset.astype(jnp.float32)[:, None, None, :]
-    log_keep = jnp.where(allowed, -jax.nn.softplus(logits), 0.0)
-    log_after = lax.cumsum(log_keep, axis=3, reverse=True) - log_keep
-    weights = jnp.where(
-        allowed, jnp.exp(jax.nn.log_sigmoid(logits) + log_after + kept_sum[..., None]), 0.0
-    )
-    weights = weights.astype(jnp.bfloat16)
-    totals = totals + jnp.einsum(
-        "grsk,kgd->grsd", weights, value_rows, preferred_element_type=jnp.float32
-    )
-    return (totals, kept_sum + jnp.sum(log_keep, axis=3))
-
-
-def mixer_half(queries, key_value, key_bias, out_weight):
-    span_rows, key_groups, pair_width = key_value.shape
+def attention_tile(q, k, v, bias, upper, kept, masked):
+    z = lax.dot_general(q, k, (((1,), (1,)), ((), ())), preferred_element_type=F32) * 0.125 + bias
+    tail = jnp.log(1.0 + jnp.exp(-jnp.abs(z)))
+    log_sig = jnp.minimum(z, 0.0) - tail
+    keep = -(jnp.maximum(z, 0.0) + tail)
+    if masked:
+        rows = lax.broadcasted_iota(jnp.int32, z.shape, 0)
+        columns = lax.broadcasted_iota(jnp.int32, z.shape, 1)
+        allowed = columns < rows
+        keep = jnp.where(allowed, keep, 0.0)
+    high = keep.astype(BF16)
+    low = (keep - high.astype(F32)).astype(BF16)
+    after = jnp.dot(high, upper, preferred_element_type=F32)
+    after = after + jnp.dot(low, upper, preferred_element_type=F32)
+    weight = jnp.exp(log_sig + after + kept)
+    if masked:
+        weight = jnp.where(allowed, weight, 0.0)
+    part = jnp.dot(weight.astype(BF16), v, preferred_element_type=F32)
+    return part, kept + jnp.sum(keep, axis=1, keepdims=True)
+
+
+def attention_kernel(place_ref, q_ref, kv_ref, bias_ref, out_ref, total, kept):
+    span, head_dim = q_ref.shape[1:]
+    spans = kv_ref.shape[0]
+    size = min(span, 256)
+    tiles = span // size
+    rows = lax.broadcasted_iota(jnp.int32, (size, size), 0)
+    columns = lax.broadcasted_iota(jnp.int32, (size, size), 1)
+    upper = jnp.where(rows > columns, 1.0, 0.0).astype(BF16)
+
+    def tile(distance, i, j, masked, state):
+        there = pl.ds(j * size, size)
+        part, after = attention_tile(
+            q_ref[0, i * size : (i + 1) * size, :],
+            kv_ref[distance, 0, there, :head_dim],
+            kv_ref[distance, 0, there, head_dim:],
+            bias_ref[distance, 0, :, there].astype(F32),
+            upper,
+            state[1],
+            masked,
+        )
+        return state[0] + part, after
+
+    for i in range(tiles):
+        state = (jnp.zeros((size, head_dim), F32), jnp.zeros((size, 1), F32))
+        for j in range(i, -1, -1):
+            state = tile(0, i, j, j == i, state)
+        total[i] = state[0]
+        kept[i] = jnp.broadcast_to(state[1], kept.shape[1:])
+    for distance in range(1, spans):
+
+        @pl.when(distance <= place_ref[0])
+        def _():
+            for i in range(tiles):
+                state = (total[i], kept[i, :, :1])
+                for j in range(tiles - 1, -1, -1):
+                    state = tile(distance, i, j, False, state)
+                total[i] = state[0]
+                kept[i] = jnp.broadcast_to(state[1], kept.shape[1:])
+
+    for i in range(tiles):
+        out_ref[0, i * size : (i + 1) * size, :] = total[i].astype(out_ref.dtype)
+
+
+def attend(queries, key_value, key_bias):
+    span, key_groups, pair_width = key_value.shape
     head_dim = pair_width // 2
-    per_group = queries.shape[1] // (key_groups * head_dim)
-    query_rows = queries.reshape(span_rows, key_groups, per_group, head_dim)
+    heads = queries.shape[1] // head_dim
+    per_group = heads // key_groups
     axis_size = lax.axis_size("ep")
     chain_length = axis_size // max(1, axis_size // 4)
-    device_place = lax.axis_index("ep")
-    chain_place = jnp.minimum((device_place + 2) % chain_length, device_place)
-    positions = jnp.arange(span_rows, dtype=jnp.int32)
-    strict_mask = positions[None, :] < positions[:, None]
-    full_mask = jnp.ones((span_rows, span_rows), dtype=bool)
-    initial = (
-        jnp.zeros((key_groups, per_group, span_rows, head_dim), jnp.float32),
-        jnp.zeros((key_groups, per_group, span_rows), jnp.float32),
+    place = lax.axis_index("ep")
+    chain_place = jnp.minimum((place + 2) % chain_length, place)
+    furthest = max(min((p + 2) % chain_length, p) for p in range(axis_size))
+    packed = jnp.concatenate([key_value.reshape(-1, pair_width), key_bias.reshape(-1, pair_width)])
+    visiting = [packed]
+    for _ in range(furthest):
+        visiting.append(passed_along(visiting[-1], "ep", 1))
+    visiting = jnp.stack(visiting)
+    keys = visiting[:, : span * key_groups].reshape(-1, span, key_groups, pair_width)
+    keys = keys.transpose(0, 2, 1, 3)
+    biases = visiting[:, span * key_groups :].reshape(-1, key_groups, 1, span)
+    size = min(span, 256)
+    attended = pl.pallas_call(
+        attention_kernel,
+        grid=(heads,),
+        out_shape=jax.ShapeDtypeStruct((heads, span, head_dim), BF16),
+        in_specs=[
+            pl.BlockSpec(memory_space=pltpu.SMEM),
+            pl.BlockSpec((1, span, head_dim), lambda h: (h, 0, 0)),
+            pl.BlockSpec((furthest + 1, 1, span, pair_width), lambda h: (0, h // per_group, 0, 0)),
+            pl.BlockSpec((furthest + 1, 1, 1, span), lambda h: (0, h // per_group, 0, 0)),
+        ],
+        out_specs=pl.BlockSpec((1, span, head_dim), lambda h: (h, 0, 0)),
+        scratch_shapes=[
+            pltpu.VMEM((span // size, size, head_dim), F32),
+            pltpu.VMEM((span // size, size, 128), F32),
+        ],
+        name="attention",
+        cost_estimate=pl.CostEstimate(flops=4 * 10**9, bytes_accessed=10**6, transcendentals=0),
+    )(
+        chain_place.reshape(1),
+        queries.reshape(span, heads, head_dim).transpose(1, 0, 2),
+        keys,
+        biases,
     )
-    running = piece_update(
-        initial,
-        query_rows,
-        key_value[..., :head_dim],
-        key_value[..., head_dim:],
-        key_bias,
-        strict_mask,
-    )
-
-    def advance(distance, loop_state):
-        current, visiting_keys, visiting_bias = loop_state
-        visiting_keys, visiting_bias = passed_along((visiting_keys, visiting_bias), "ep", 1)
-
-        def include(earlier_state):
-            return piece_update(
-                earlier_state,
-                query_rows,
-                visiting_keys[..., :head_dim],
-                visiting_keys[..., head_dim:],
-                visiting_bias,
-                full_mask,
+    return attended.transpose(1, 0, 2).reshape(span, heads * head_dim)
+
+
+def project(attended, out_weight):
+    return jnp.dot(attended, out_weight, preferred_element_type=F32).astype(BF16)
+
+
+def exchange_kernel(
+    capacity,
+    terms_ref,
+    normed_ref,
+    meta_ref,
+    shared_gate,
+    shared_up,
+    shared_down,
+    gate_hbm,
+    up_hbm,
+    down_hbm,
+    mixer_ref,
+    expert_ref,
+    gathered,
+    meta,
+    gate_v,
+    up_v,
+    down_v,
+    chosen,
+    shared,
+    sums,
+    from_sibling,
+    from_side,
+    from_line,
+    mixer_sibling,
+    mixer_side,
+    mixer_sum,
+    load_sem,
+    meta_send,
+    meta_recv,
+    zs_send,
+    zs_recv,
+    x_send,
+    x_recv,
+    s_send,
+    s_recv,
+    rz_send,
+    rz_recv,
+    rx_send,
+    rx_recv,
+    rs_send,
+    rs_recv,
+    m_send,
+    m_recv,
+):
+    count = lax.axis_size("ep")
+    width = normed_ref.shape[1]
+    tokens = normed_ref.shape[0]
+    half = width // 2
+    z = lax.axis_index("ep")
+    t = lax.axis_index("tp")
+    x, c = t // 2, t % 2
+    ox, oc = 1 - x, 1 - c
+    side, sibling = ox * 2 + c, x * 2 + oc
+    group = count * 4
+    me = z * 4 + t
+
+    loads = [
+        pltpu.make_async_copy(a, b, load_sem.at[i])
+        for i, (a, b) in enumerate(((gate_hbm, gate_v), (up_hbm, up_v), (down_hbm, down_v)))
+    ]
+    own_load = pltpu.make_async_copy(normed_ref, gathered.at[z, x, c], load_sem.at[3])
+    own_meta = pltpu.make_async_copy(meta_ref.at[me], meta.at[me], load_sem.at[4])
+    own_load.start()
+    own_meta.start()
+
+    barrier = pltpu.get_barrier_semaphore()
+    for step in range(1, group):
+        other = (me + step) % group
+        pl.semaphore_signal(
+            barrier, 1, device_id={"ep": other // 4, "tp": other % 4}, device_id_type=MESH
+        )
+    pl.semaphore_wait(barrier, group - 1)
+
+    def copy(src, dst, send, recv, ep, tp):
+        return pltpu.make_async_remote_copy(
+            src_ref=src,
+            dst_ref=dst,
+            send_sem=send,
+            recv_sem=recv,
+            device_id={"ep": ep, "tp": tp},
+            device_id_type=MESH,
+        )
+
+    own_load.wait()
+    own_meta.wait()
+
+    def part(zz, xx, cc, h):
+        return gathered.at[zz, xx, cc, :, pl.ds(h * half, half)]
+
+    def line(up, kind, zz):
+        block = part(zz, ox if kind == 1 else x, c, 1 if kind == 2 else 0)
+        return copy(
+            block,
+            block,
+            zs_send.at[0 if up else 1, kind, zz],
+            zs_recv.at[kind, zz],
+            z + (1 if up else -1),
+            t,
+        )
+
+    def across(slot, zz):
+        block = part(zz, x, c, 0 if slot == 0 else 1)
+        index = 0 if slot == 0 else 1 + zz
+        return copy(block, block, x_send.at[index], x_recv.at[index], z, side)
+
+    def across_in(slot, zz):
+        block = part(zz, ox, c, 0 if slot == 0 else 1)
+        index = 0 if slot == 0 else 1 + zz
+        return copy(block, block, x_send.at[index], x_recv.at[index], z, side)
+
+    def share(zz, xx, h):
+        block = part(zz, xx, c, h)
+        return copy(block, block, s_send.at[zz, xx, h], s_recv.at[zz, xx, h], z, sibling)
+
+    def share_in(zz, xx, h):
+        block = part(zz, xx, oc, h)
+        return copy(block, block, s_send.at[zz, xx, h], s_recv.at[zz, xx, h], z, sibling)
+
+    def meta_copy(step):
+        other = (me + step) % group
+        return copy(
+            meta_ref.at[other],
+            meta.at[me],
+            meta_send.at[step - 1],
+            meta_recv.at[step - 1],
+            other // 4,
+            other % 4,
+        )
+
+    def meta_in(step):
+        other = (me + group - step) % group
+        return copy(
+            meta_ref.at[other],
+            meta.at[other],
+            meta_send.at[step - 1],
+            meta_recv.at[step - 1],
+            other // 4,
+            other % 4,
+        )
+
+    can_up, can_down = z + 1 < count, z >= 1
+
+    across(0, z).start()
+    for kind in (0, 2):
+
+        @pl.when(can_up)
+        def _():
+            line(True, kind, z).start()
+
+        @pl.when(can_down)
+        def _():
+            line(False, kind, z).start()
+
+    across(1, z).start()
+    for step in range(1, group):
+        meta_copy(step).start()
+    share(z, x, 0).start()
+    share(z, x, 1).start()
+    for load in loads:
+        load.start()
+
+    def mixer_pair(xx):
+        return copy(
+            terms_ref.at[xx, oc],
+            mixer_sibling.at[xx],
+            m_send.at[xx],
+            m_recv.at[xx],
+            z,
+            sibling,
+        )
+
+    for xx in range(2):
+        mixer_pair(xx).start()
+
+    across_in(0, z).wait_recv()
+
+    @pl.when(can_up)
+    def _():
+        line(True, 1, z).start()
+
+    @pl.when(can_down)
+    def _():
+        line(False, 1, z).start()
+
+    share(z, ox, 0).start()
+
+    hidden_gate = jnp.dot(normed_ref[...], shared_gate[...], preferred_element_type=F32)
+    hidden_up = jnp.dot(normed_ref[...], shared_up[...], preferred_element_type=F32)
+    shared_hidden = (hidden_gate / (1.0 + jnp.exp(-hidden_gate)) * hidden_up).astype(BF16)
+    shared[...] = jnp.dot(shared_hidden, shared_down[...], preferred_element_type=F32)
+
+    for distance in range(1, count):
+        below, above = z - distance, z + distance
+
+        def arrive(kind, zz, going_up, further):
+            line(going_up, kind, zz).wait_recv()
+
+            @pl.when(further)
+            def _():
+                line(going_up, kind, zz).start()
+
+            if kind == 2:
+                across(1, zz).start()
+            share(zz, ox if kind == 1 else x, 1 if kind == 2 else 0).start()
+
+        for kind in (0, 2, 1):
+
+            @pl.when(below >= 0)
+            def _():
+                arrive(kind, below, True, can_up)
+
+            @pl.when(above < count)
+            def _():
+                arrive(kind, above, False, can_down)
+
+    for xx in range(2):
+        mixer_pair(xx).wait()
+    mixer_sum[...] = (
+        terms_ref[ox, c].astype(F32) + mixer_sibling[ox].astype(F32)
+    ).astype(BF16)
+    mixer_move = copy(mixer_sum, mixer_side, m_send.at[2], m_recv.at[2], z, side)
+    mixer_move.start()
+
+    for step in range(count):
+        zz = (z + step) % count
+        across_in(1, zz).wait_recv()
+        share(zz, ox, 1).start()
+    for step in range(1, group):
+        meta_in(step).wait_recv()
+    for zz in range(count):
+        for xx in range(2):
+            for h in range(2):
+                share_in(zz, xx, h).wait_recv()
+    for load in loads:
+        load.wait()
+
+    batch = chosen.shape[0] // capacity
+    slots = lax.broadcasted_iota(jnp.int32, (capacity, tokens), 0).astype(F32)
+
+    def picker(source):
+        return jnp.where(meta[source, 1:2, :] == slots, 1.0, 0.0)
+
+    @pl.loop(0, group // batch)
+    def _(turn):
+        for i in range(batch):
+            source = turn * batch + i
+            block = gathered[source // 4, (source % 4) // 2, source % 2]
+            chosen[i * capacity : (i + 1) * capacity, :] = jnp.dot(
+                picker(source).astype(BF16), block, preferred_element_type=F32
+            ).astype(BF16)
+        gate = jnp.dot(chosen[...], gate_v[...], preferred_element_type=F32)
+        up = jnp.dot(chosen[...], up_v[...], preferred_element_type=F32)
+        hidden = (gate / (1.0 + jnp.exp(-gate)) * up).astype(BF16)
+        for i in range(batch):
+            source = turn * batch + i
+            pick = picker(source)
+            scale = jnp.sum(pick * meta[source, 0:1, :], axis=1, keepdims=True)
+            rows = jnp.dot(
+                hidden[i * capacity : (i + 1) * capacity, :],
+                down_v[...],
+                preferred_element_type=F32,
             )
-
-        def skip(earlier_state):
-            return earlier_state
-
-        current = lax.cond(distance <= chain_place, include, skip, current)
-        return (current, visiting_keys, visiting_bias)
-
-    running, _, _ = lax.fori_loop(1, chain_length, advance, (running, key_value, key_bias))
-    attended = running[0].astype(jnp.bfloat16)
-    projection = out_weight.reshape(key_groups, per_group, head_dim, out_weight.shape[1])
-    return lax.psum_scatter(
-        jnp.einsum(
-            "grsd,grde->se", attended, projection, preferred_element_type=jnp.float32
-        ).astype(jnp.bfloat16),
-        "tp",
-        scatter_dimension=0,
-        tiled=True,
-    )
+            rows = (rows * scale).astype(BF16)
+            sums[source // 4, (source % 4) // 2, source % 2] = lax.dot_general(
+                pick.astype(BF16), rows, (((0,), (0,)), ((), ())), preferred_element_type=F32
+            ).astype(BF16)
+
+    def pair(zz, xx):
+        return copy(
+            sums.at[zz, xx, oc],
+            from_sibling.at[zz, xx],
+            rs_send.at[zz, xx],
+            rs_recv.at[zz, xx],
+            z,
+            sibling,
+        )
+
+    def half_ref(zz, xx, h):
+        return sums.at[zz, xx, c, :, pl.ds(h * half, half)]
+
+    def side_move(zz):
+        return copy(
+            half_ref(zz, ox, 1), from_side.at[1 + zz], rx_send.at[1 + zz], rx_recv.at[1 + zz], z, side
+        )
+
+    def last_move():
+        return copy(half_ref(z, ox, 0), from_side.at[0], rx_send.at[0], rx_recv.at[0], z, side)
+
+    def back(up, kind, zz):
+        return copy(
+            half_ref(zz, ox if kind == 1 else x, 1 if kind == 2 else 0),
+            from_line.at[0 if up else 1, kind, zz],
+            rz_send.at[kind, zz],
+            rz_recv.at[0 if up else 1, kind, zz],
+            z + (1 if up else -1),
+            t,
+        )
+
+    def add(ref, other):
+        ref[...] = (ref[...].astype(F32) + other[...].astype(F32)).astype(BF16)
+
+    order = []
+    for step in range(count):
+        order.append((z + count // 2 + step) % count)
+    for zz in order:
+        for xx in (ox, x):
+            pair(zz, xx).start()
+    for zz in order:
+        for xx in (ox, x):
+            pair(zz, xx).wait_recv()
+            add(sums.at[zz, xx, c], from_sibling.at[zz, xx])
+        side_move(zz).start()
+
+    for distance in range(count - 1, 0, -1):
+        for kind in (0, 1, 2):
+            for up in (True, False):
+                target = z + distance if up else z - distance
+                exists = target < count if up else target >= 0
+                feeds = can_down if up else can_up
+
+                @pl.when(exists)
+                def _():
+                    mine = half_ref(target, ox if kind == 1 else x, 1 if kind == 2 else 0)
+                    if kind == 2:
+                        side_move(target).wait_recv()
+                        add(mine, from_side.at[1 + target])
+
+                    @pl.when(feeds)
+                    def _():
+                        back(up, kind, target).wait_recv()
+                        add(mine, from_line.at[0 if up else 1, kind, target])
+
+                    back(up, kind, target).start()
+
+    for kind in (1, 0, 2):
+        mine = half_ref(z, ox if kind == 1 else x, 1 if kind == 2 else 0)
+        if kind == 2:
+            side_move(z).wait_recv()
+            add(mine, from_side.at[1 + z])
+        for up in (True, False):
+
+            @pl.when(can_down if up else can_up)
+            def _():
+                back(up, kind, z).wait_recv()
+                add(mine, from_line.at[0 if up else 1, kind, z])
+
+        if kind == 1:
+            last_move().start()
+
+    mixer_move.wait()
+    mixer_ref[...] = (
+        terms_ref[x, c].astype(F32)
+        + mixer_sibling[x].astype(F32)
+        + mixer_side[...].astype(F32)
+    ).astype(BF16)
+    expert_ref[:, half:] = (sums[z, x, c, :, half:].astype(F32) + shared[:, half:]).astype(BF16)
+    last_move().wait_recv()
+    expert_ref[:, :half] = (
+        sums[z, x, c, :, :half].astype(F32) + from_side[0].astype(F32) + shared[:, :half]
+    ).astype(BF16)
+
+    for step in range(1, group):
+        meta_copy(step).wait_send()
+    across(0, z).wait_send()
+    last_move().wait_send()
+    for zz in range(count):
+        across(1, zz).wait_send()
+        side_move(zz).wait_send()
+        for xx in range(2):
+            pair(zz, xx).wait_send()
+            for h in range(2):
+                share(zz, xx, h).wait_send()
+        for kind in range(3):
+
+            @pl.when((zz <= z) & can_up)
+            def _():
+                line(True, kind, zz).wait_send()
+
+            @pl.when((zz >= z) & can_down)
+            def _():
+                line(False, kind, zz).wait_send()
+
+            @pl.when(zz > z)
+            def _():
+                back(True, kind, zz).wait_send()
+
+            @pl.when(zz < z)
+            def _():
+                back(False, kind, zz).wait_send()
+
+
+def exchange(terms, normed, meta, shared_parts, routed_parts, capacity):
+    tokens, width = normed.shape
+    count = lax.axis_size("ep")
+    group = count * 4
+    hidden = routed_parts[0].shape[1]
+    half = width // 2
+    batch = 8 if group % 8 == 0 else 4
+    dma = pltpu.SemaphoreType.DMA
+    vmem = pl.BlockSpec(memory_space=pltpu.VMEM)
+    return pl.pallas_call(
+        lambda *refs: exchange_kernel(capacity, *refs),
+        out_shape=[jax.ShapeDtypeStruct((tokens, width), BF16)] * 2,
+        in_specs=[vmem] * 6 + [pl.BlockSpec(memory_space=pl.ANY)] * 3,
+        out_specs=[vmem] * 2,
+        scratch_shapes=[
+            pltpu.VMEM((count, 2, 2, tokens, width), BF16),
+            pltpu.VMEM(meta.shape, F32),
+            pltpu.VMEM((width, hidden), BF16),
+            pltpu.VMEM((width, hidden), BF16),
+            pltpu.VMEM((hidden, width), BF16),
+            pltpu.VMEM((batch * capacity, width), BF16),
+            pltpu.VMEM((tokens, width), F32),
+            pltpu.VMEM((count, 2, 2, tokens, width), BF16),
+            pltpu.VMEM((count, 2, tokens, width), BF16),
+            pltpu.VMEM((1 + count, tokens, half), BF16),
+            pltpu.VMEM((2, 3, count, tokens, half), BF16),
+            pltpu.VMEM((2, tokens, width), BF16),
+            pltpu.VMEM((tokens, width), BF16),
+            pltpu.VMEM((tokens, width), BF16),
+            dma((5,)),
+            dma((group - 1,)),
+            dma((group - 1,)),
+            dma((2, 3, count)),
+            dma((3, count)),
+            dma((1 + count,)),
+            dma((1 + count,)),
+            dma((count, 2, 2)),
+            dma((count, 2, 2)),
+            dma((3, count)),
+            dma((2, 3, count)),
+            dma((1 + count,)),
+            dma((1 + count,)),
+            dma((count, 2)),
+            dma((count, 2)),
+            dma((3,)),
+            dma((3,)),
+        ],
+        compiler_params=pltpu.CompilerParams(
+            collective_id=0, has_side_effects=True, vmem_limit_bytes=60 * 2**20
+        ),
+        name="exchange",
+        cost_estimate=pl.CostEstimate(flops=10**10, bytes_accessed=2 * 10**7, transcendentals=0),
+    )(terms.reshape(2, 2, tokens, width), normed, meta, *shared_parts, *routed_parts)
+
+
+def normalise(expert_input, norm_gain):
+    widened = expert_input.astype(F32)
+    return (
+        widened * lax.rsqrt(jnp.mean(widened * widened, axis=-1, keepdims=True) + 1e-06) * norm_gain
+    ).astype(BF16)
+
+
+def route_table(routes, route_weights, experts):
+    tokens = routes.shape[0]
+    named = routes[:, None, :] == jnp.arange(experts, dtype=jnp.int32)[None, :, None]
+    weight = jnp.sum(jnp.where(named, route_weights[:, None, :], 0.0), axis=2)
+    chosen = jnp.any(named, axis=2)
+    earlier = jnp.arange(tokens)[None, :] < jnp.arange(tokens)[:, None]
+    slot = jnp.dot(earlier.astype(BF16), chosen.astype(BF16), preferred_element_type=F32)
+    slot = jnp.where(chosen, slot, -1.0)
+    table = jnp.stack([weight.T, slot.T], axis=1)
+    return jnp.pad(table, ((0, 0), (0, 6), (0, 0)))
 
 
 def expert_rows(arrived, gate_weight, up_weight, down_weight):
@@ -173,7 +681,23 @@
     shared_up,
     shared_down,
 ):
-    mixer_output = mixer_half(queries, key_value, key_bias, out_weight)
+    terms = project(attend(queries, key_value, key_bias), out_weight)
+    tokens, top_count = routes.shape
+    width = expert_input.shape[1]
+    tp_count = lax.axis_size("tp")
+    experts = lax.axis_size("ep") * tp_count
+    if tp_count == 4 and experts * tokens * width * 2 <= 8 * 2**20:
+        capacity = max(2, 3 * tokens * top_count // (2 * experts))
+        mixer_output, expert_output = exchange(
+            terms,
+            normalise(expert_input, norm_gain),
+            route_table(routes, route_weights, experts),
+            (shared_gate, shared_up, shared_down),
+            (gate_weight[0], up_weight[0], down_weight[0]),
+            capacity,
+        )
+        return (mixer_output, expert_output)
+    mixer_output = lax.psum_scatter(terms, "tp", scatter_dimension=0, tiled=True)
     expert_output = experts_half(
         expert_input,
         norm_gain,

time: 271 us -> 177 us (0.65)
  the two profiles are of different devices: /device:TPU:0 before, /device:TPU:16 now
where the time goes in v1:
time: 177 us
  Pallas kernels  156 us (88%)
  other arithmetic  7.79 us (4%)
  local copies, waits for them, and re-layouts  6.43 us (4%)
  starting transfers between devices  3.48 us (2%)
  matrix products  2.24 us (1%)
    pallas_call x1, Pallas kernels, exchange(): pl.pallas_call(lambda *refs: exchange_kernel(capacity, *refs), out_shape=...  150 us
    pallas_call x1, Pallas kernels, attend(): pl.pallas_call(attention_kernel, grid=(heads,), out_shape=jax.ShapeDtypeS...  5.59 us
    unnamed x6, local copies, waits for them, and re-layouts  3.78 us
  transfers between devices with their start and end apart: 1, of which 0 were waited for; matrix products, arithmetic and copies ran while one was open for 4% of the time, Pallas kernels for 0%

profile of v1, /device:TPU:16, one launch (start us, length us, event | category | flops | bytes accessed | tf_op | source)
XLA Modules:
  0.0 176.6 jit_solution(6341063864209720064)
XLA Ops:
  0.6 0.0 copy-start
  0.6 0.0 copy-start.1
  0.7 0.8 reduce
  1.4 0.9 pad_maximum_fusion
  2.4 3.5 %collective-permute-start = (bf16[516,128]{1,0:T(8,128)(2,1)S(1)}, bf16[516,128]{1,0:T(8,128)(2,1)S(1)}, u32[]{:S(2)}, u32[]{:S(2)}) collective-permute-start(bf16[516,128]{1,0:T(8,128)(2,1)S(1)} %get-tuple-element.2), channel_id=1, source_target_pairs={{0,4},{4,8},{8,12},{1,5},{5,9},{9,13},{2,6},{6,10},{10,14},{3,7},{... | collective-permute-start | bytes 396296 | tf_op jit(solution)/shard_map/ppermute | solution.py:16
  5.9 1.2 fusion
  7.1 0.7 fusion.5
  7.8 0.1 convolution_select_fusion
  8.0 2.0 %fusion.2.refs_1_ = bf16[128,2048]{1,0:T(8,128)(2,1)} fusion(bf16[128,2048]{1,0:T(8,128)(2,1)} %param.18, f32[2048]{0:T(1024)} %param.19, f32[128]{0:T(128)S(1)} %add_rsqrt_fusion), kind=kLoop, calls=%fused_computation.6 | loop fusion | flops 1048576 | bytes 1057280 | tf_op jit(solution)/shard_map/convert_element_type | solution.py:583
  10.0 0.7 select_reduce_fusion
  10.7 0.0 copy-done.1
  10.7 0.9 copy.23
  11.7 0.6 select_maximum_fusion.refs_2_
  12.3 0.0 collective-permute-done
  12.3 0.7 fusion.4.kv_ref
  13.0 0.6 reshape.43.bias_ref
  13.6 5.6 %attention.1 = bf16[3,512,64]{2,1,0:T(8,128)(2,1)} custom-call(s32[1]{0:T(128)} %bitcast.place_ref, bf16[3,512,64]{2,1,0:T(8,128)(2,1)} %bitcast.29, bf16[2,1,512,128]{3,2,1,0:T(8,128)(2,1)} %fusion.4.kv_ref, bf16[2,1,1,512]{3,2,1,0:T(2,128)(2,1)} %reshape.43.bias_ref), custom_call_target="tpu_custom_call" | custom-call | flops 4000000000 | bytes 1000000 | tf_op jit(solution)/shard_map/attention/pallas_call | solution.py:102
  19.2 1.1 copy.25
  20.4 0.0 copy-done
  20.4 2.1 %convolution_convert_fusion = bf16[512,2048]{1,0:T(8,128)(2,1)} fusion(bf16[512,192]{0,1:T(8,128)(2,1)S(1)} %bitcast.26, bf16[192,2048]{1,0:T(8,128)(2,1)S(1)} %copy-done), kind=kOutput, calls=%fused_computation | convolution fusion | flops 403701760 | bytes 3080192 | tf_op jit(solution)/shard_map/dot_general | solution.py:129
  22.5 150.4 %exchange.1 = (bf16[128,2048]{1,0:T(8,128)(2,1)}, bf16[128,2048]{1,0:T(8,128)(2,1)}) custom-call(bf16[2,2,128,2048]{3,2,1,0:T(8,128)(2,1)} %bitcast.25, bf16[128,2048]{1,0:T(8,128)(2,1)} %fusion.2.refs_1_, f32[16,8,128]{2,1,0:T(8,128)} %select_maximum_fusion.refs_2_, bf16[2048,256]{1,0:T(8,128)(2,1)} %refs_3_.1, bf16[2048,256]{1,0:T(8,128)(2,1)} %refs_4_.1, ...), custom_call_target="tpu_custom_call" | custom-call | flops 10000000000 | bytes 20000000 | tf_op jit(solution)/shard_map/exchange/pallas_call | solution.py:533
  172.9 1.9 %copy.28 = bf16[128,2048]{1,0:T(8,128)(2,1)} copy(bf16[128,2048]{1,0:T(8,128)(2,1)} %get-tuple-element.6) | data formatting | bytes 1048576
  174.7 1.9 %copy.29 = bf16[128,2048]{1,0:T(8,128)(2,1)} copy(bf16[128,2048]{1,0:T(8,128)(2,1)} %get-tuple-element.7) | data formatting | bytes 1048576
  (2 shorter events, 0.0 us)
Async XLA Ops:
  0.6 19.7 %copy-start = (bf16[192,2048]{1,0:T(8,128)(2,1)S(1)}, bf16[192,2048]{1,0:T(8,128)(2,1)}, u32[]{:S(2)}) copy-start(bf16[192,2048]{1,0:T(8,128)(2,1)} %param.17) | copy-start | bytes 2359300
  0.6 10.1 %copy-start.1 = (bf16[512,192]{0,1:T(8,128)(2,1)S(1)}, bf16[512,192]{0,1:T(8,128)(2,1)}, u32[]{:S(2)}) copy-start(bf16[512,192]{0,1:T(8,128)(2,1)} %param.14) | copy-start | bytes 589828
  2.4 9.9 %collective-permute-start = (bf16[516,128]{1,0:T(8,128)(2,1)S(1)}, bf16[516,128]{1,0:T(8,128)(2,1)S(1)}, u32[]{:S(2)}, u32[]{:S(2)}) collective-permute-start(bf16[516,128]{1,0:T(8,128)(2,1)S(1)} %get-tuple-element.2), channel_id=1, source_target_pairs={{0,4},{4,8},{8,12},{1,5},{5,9},{9,13},{2,6},{6,10},{10,14},{3,7},{... | collective-permute-start | bytes 396296 | tf_op jit(solution)/shard_map/ppermute | solution.py:16

commit v2 on v1

--- a/solution.py
+++ b/solution.py
@@ -131,6 +131,7 @@
 
 def exchange_kernel(
     capacity,
+    batch,
     terms_ref,
     normed_ref,
     meta_ref,
@@ -177,7 +178,9 @@
     count = lax.axis_size("ep")
     width = normed_ref.shape[1]
     tokens = normed_ref.shape[0]
-    half = width // 2
+    cut = width // 4
+    spans = (slice(0, cut), slice(cut, width))
+    pieces = (pl.ds(0, cut), pl.ds(cut, width - cut))
     z = lax.axis_index("ep")
     t = lax.axis_index("tp")
     x, c = t // 2, t % 2
@@ -217,7 +220,7 @@
     own_meta.wait()
 
     def part(zz, xx, cc, h):
-        return gathered.at[zz, xx, cc, :, pl.ds(h * half, half)]
+        return gathered.at[zz, xx, cc, :, pieces[h]]
 
     def line(up, kind, zz):
         block = part(zz, ox if kind == 1 else x, c, 1 if kind == 2 else 0)
@@ -271,9 +274,30 @@
         )
 
     can_up, can_down = z + 1 < count, z >= 1
+    slots = lax.broadcasted_iota(jnp.int32, (capacity, tokens), 0).astype(F32)
+
+    def picker(source):
+        return jnp.where(meta[source, 1:2, :] == slots, 1.0, 0.0)
+
+    def rows_of(source):
+        return pl.ds(pl.multiple_of(source * capacity, 16), capacity)
+
+    def pick(zz, xx, cc, h):
+        source = zz * 4 + xx * 2 + cc
+        columns = spans[h]
+        chosen[rows_of(source), columns] = jnp.dot(
+            picker(source).astype(BF16),
+            gathered[zz, xx, cc, :, columns],
+            preferred_element_type=F32,
+        ).astype(BF16)
+
+    def pick_both(zz, xx, h):
+        pick(zz, xx, c, h)
+        share_in(zz, xx, h).wait_recv()
+        pick(zz, xx, oc, h)
 
     across(0, z).start()
-    for kind in (0, 2):
+    for kind in (2, 0):
 
         @pl.when(can_up)
         def _():
@@ -304,23 +328,33 @@
     for xx in range(2):
         mixer_pair(xx).start()
 
-    across_in(0, z).wait_recv()
-
-    @pl.when(can_up)
-    def _():
-        line(True, 1, z).start()
-
-    @pl.when(can_down)
-    def _():
-        line(False, 1, z).start()
-
-    share(z, ox, 0).start()
-
     hidden_gate = jnp.dot(normed_ref[...], shared_gate[...], preferred_element_type=F32)
     hidden_up = jnp.dot(normed_ref[...], shared_up[...], preferred_element_type=F32)
     shared_hidden = (hidden_gate / (1.0 + jnp.exp(-hidden_gate)) * hidden_up).astype(BF16)
     shared[...] = jnp.dot(shared_hidden, shared_down[...], preferred_element_type=F32)
 
+    across_in(0, z).wait_recv()
+
+    @pl.when(can_up)
+    def _():
+        line(True, 1, z).start()
+
+    @pl.when(can_down)
+    def _():
+        line(False, 1, z).start()
+
+    share(z, ox, 0).start()
+    for step in range(1, group):
+        meta_in(step).wait_recv()
+    pick_both(z, x, 0)
+    pick_both(z, x, 1)
+    pick_both(z, ox, 0)
+
+    def other_side(zz):
+        across_in(1, zz).wait_recv()
+        share(zz, ox, 1).start()
+        pick_both(zz, ox, 1)
+
     for distance in range(1, count):
         below, above = z - distance, z + distance
 
@@ -335,7 +369,7 @@
                 across(1, zz).start()
             share(zz, ox if kind == 1 else x, 1 if kind == 2 else 0).start()
 
-        for kind in (0, 2, 1):
+        for kind in (2, 0, 1):
 
             @pl.when(below >= 0)
             def _():
@@ -344,6 +378,22 @@
             @pl.when(above < count)
             def _():
                 arrive(kind, above, False, can_down)
+
+            for there, zz in ((below >= 0, below), (above < count, above)):
+
+                @pl.when(there)
+                def _():
+                    pick_both(zz, ox if kind == 1 else x, 1 if kind == 2 else 0)
+
+        for there, zz in (
+            ((z >= 0, z),)
+            if distance == 1
+            else ((below + 1 >= 0, below + 1), (above - 1 < count, above - 1))
+        ):
+
+            @pl.when(there)
+            def _():
+                other_side(zz)
 
     for xx in range(2):
         mixer_pair(xx).wait()
@@ -353,49 +403,39 @@
     mixer_move = copy(mixer_sum, mixer_side, m_send.at[2], m_recv.at[2], z, side)
     mixer_move.start()
 
-    for step in range(count):
-        zz = (z + step) % count
-        across_in(1, zz).wait_recv()
-        share(zz, ox, 1).start()
-    for step in range(1, group):
-        meta_in(step).wait_recv()
-    for zz in range(count):
-        for xx in range(2):
-            for h in range(2):
-                share_in(zz, xx, h).wait_recv()
+    for zz in (z - (count - 1), z + (count - 1)):
+
+        @pl.when((zz >= 0) & (zz < count))
+        def _():
+            other_side(zz)
+
     for load in loads:
         load.wait()
 
-    batch = chosen.shape[0] // capacity
-    slots = lax.broadcasted_iota(jnp.int32, (capacity, tokens), 0).astype(F32)
-
-    def picker(source):
-        return jnp.where(meta[source, 1:2, :] == slots, 1.0, 0.0)
-
     @pl.loop(0, group // batch)
     def _(turn):
+        block = pl.ds(pl.multiple_of(turn * (batch * capacity), 16), batch * capacity)
+        scales = []
         for i in range(batch):
             source = turn * batch + i
-            block = gathered[source // 4, (source % 4) // 2, source % 2]
-            chosen[i * capacity : (i + 1) * capacity, :] = jnp.dot(
-                picker(source).astype(BF16), block, preferred_element_type=F32
-            ).astype(BF16)
-        gate = jnp.dot(chosen[...], gate_v[...], preferred_element_type=F32)
-        up = jnp.dot(chosen[...], up_v[...], preferred_element_type=F32)
+            scales.append(
+                jnp.sum(picker(source) * meta[source, 0:1, :], axis=1, keepdims=True)
+            )
+        scale = jnp.concatenate(scales, axis=0)
+        gate = jnp.dot(chosen[block, :], gate_v[...], preferred_element_type=F32)
+        up = jnp.dot(chosen[block, :], up_v[...], preferred_element_type=F32)
         hidden = (gate / (1.0 + jnp.exp(-gate)) * up).astype(BF16)
-        for i in range(batch):
-            source = turn * batch + i
-            pick = picker(source)
-            scale = jnp.sum(pick * meta[source, 0:1, :], axis=1, keepdims=True)
-            rows = jnp.dot(
-                hidden[i * capacity : (i + 1) * capacity, :],
-                down_v[...],
-                preferred_element_type=F32,
-            )
-            rows = (rows * scale).astype(BF16)
-            sums[source // 4, (source % 4) // 2, source % 2] = lax.dot_general(
-                pick.astype(BF16), rows, (((0,), (0,)), ((), ())), preferred_element_type=F32
-            ).astype(BF16)
+        rows = jnp.dot(hidden, down_v[...], preferred_element_type=F32)
+        chosen[block, :] = (rows * scale).astype(BF16)
+
+    def spread(zz, xx, cc):
+        source = zz * 4 + xx * 2 + cc
+        sums[zz, xx, cc] = lax.dot_general(
+            picker(source).astype(BF16),
+            chosen[rows_of(source), :],
+            (((0,), (0,)), ((), ())),
+            preferred_element_type=F32,
+        ).astype(BF16)
 
     def pair(zz, xx):
         return copy(
@@ -408,20 +448,27 @@
         )
 
     def half_ref(zz, xx, h):
-        return sums.at[zz, xx, c, :, pl.ds(h * half, half)]
+        return sums.at[zz, xx, c, :, pieces[h]]
+
+    def side_ref(h, zz):
+        return from_side.at[1 + zz] if h else from_side.at[0, :, pieces[0]]
+
+    def line_ref(up, kind, zz):
+        slot = from_line.at[0 if up else 1, kind, zz]
+        return slot if kind == 2 else slot.at[:, pieces[0]]
 
     def side_move(zz):
         return copy(
-            half_ref(zz, ox, 1), from_side.at[1 + zz], rx_send.at[1 + zz], rx_recv.at[1 + zz], z, side
+            half_ref(zz, ox, 1), side_ref(1, zz), rx_send.at[1 + zz], rx_recv.at[1 + zz], z, side
         )
 
     def last_move():
-        return copy(half_ref(z, ox, 0), from_side.at[0], rx_send.at[0], rx_recv.at[0], z, side)
+        return copy(half_ref(z, ox, 0), side_ref(0, z), rx_send.at[0], rx_recv.at[0], z, side)
 
     def back(up, kind, zz):
         return copy(
             half_ref(zz, ox if kind == 1 else x, 1 if kind == 2 else 0),
-            from_line.at[0 if up else 1, kind, zz],
+            line_ref(up, kind, zz),
             rz_send.at[kind, zz],
             rz_recv.at[0 if up else 1, kind, zz],
             z + (1 if up else -1),
@@ -432,19 +479,37 @@
         ref[...] = (ref[...].astype(F32) + other[...].astype(F32)).astype(BF16)
 
     order = []
-    for step in range(count):
-        order.append((z + count // 2 + step) % count)
-    for zz in order:
-        for xx in (ox, x):
-            pair(zz, xx).start()
-    for zz in order:
+    for k in range(count - 1):
+        low = (count - 1 - k) - (z - (count - 1 - k) + count) // count
+        high = k + (k - z + count) // count
+        order.append(low + (z // (count // 2)) * (high - low))
+    order.append(z)
+
+    def finish(zz, own):
         for xx in (ox, x):
             pair(zz, xx).wait_recv()
             add(sums.at[zz, xx, c], from_sibling.at[zz, xx])
         side_move(zz).start()
+        if not own:
+            for up, edge in ((True, z == 0), (False, z == count - 1)):
+
+                @pl.when(edge)
+                def _():
+                    back(up, 1, zz).start()
+                    back(up, 0, zz).start()
+
+    for k in range(count + 1):
+        if k < count:
+            for xx in (ox, x):
+                spread(order[k], xx, oc)
+                pair(order[k], xx).start()
+            for xx in (ox, x):
+                spread(order[k], xx, c)
+        if k >= 1:
+            finish(order[k - 1], k == count)
 
     for distance in range(count - 1, 0, -1):
-        for kind in (0, 1, 2):
+        for kind in (1, 0, 2):
             for up in (True, False):
                 target = z + distance if up else z - distance
                 exists = target < count if up else target >= 0
@@ -460,9 +525,12 @@
                     @pl.when(feeds)
                     def _():
                         back(up, kind, target).wait_recv()
-                        add(mine, from_line.at[0 if up else 1, kind, target])
-
-                    back(up, kind, target).start()
+                        add(mine, line_ref(up, kind, target))
+                        if kind != 2:
+                            back(up, kind, target).start()
+
+                    if kind == 2:
+                        back(up, kind, target).start()
 
     for kind in (1, 0, 2):
         mine = half_ref(z, ox if kind == 1 else x, 1 if kind == 2 else 0)
@@ -474,7 +542,7 @@
             @pl.when(can_down if up else can_up)
             def _():
                 back(up, kind, z).wait_recv()
-                add(mine, from_line.at[0 if up else 1, kind, z])
+                add(mine, line_ref(up, kind, z))
 
         if kind == 1:
             last_move().start()
@@ -485,10 +553,10 @@
         + mixer_sibling[x].astype(F32)
         + mixer_side[...].astype(F32)
     ).astype(BF16)
-    expert_ref[:, half:] = (sums[z, x, c, :, half:].astype(F32) + shared[:, half:]).astype(BF16)
+    expert_ref[:, cut:] = (sums[z, x, c, :, cut:].astype(F32) + shared[:, cut:]).astype(BF16)
     last_move().wait_recv()
-    expert_ref[:, :half] = (
-        sums[z, x, c, :, :half].astype(F32) + from_side[0].astype(F32) + shared[:, :half]
+    expert_ref[:, :cut] = (
+        sums[z, x, c, :, :cut].astype(F32) + from_side[0, :, :cut].astype(F32) + shared[:, :cut]
     ).astype(BF16)
 
     for step in range(1, group):
@@ -526,12 +594,12 @@
     count = lax.axis_size("ep")
     group = count * 4
     hidden = routed_parts[0].shape[1]
-    half = width // 2
+    rest = width - width // 4
     batch = 8 if group % 8 == 0 else 4
     dma = pltpu.SemaphoreType.DMA
     vmem = pl.BlockSpec(memory_space=pltpu.VMEM)
     return pl.pallas_call(
-        lambda *refs: exchange_kernel(capacity, *refs),
+        lambda *refs: exchange_kernel(capacity, batch, *refs),
         out_shape=[jax.ShapeDtypeStruct((tokens, width), BF16)] * 2,
         in_specs=[vmem] * 6 + [pl.BlockSpec(memory_space=pl.ANY)] * 3,
         out_specs=[vmem] * 2,
@@ -541,12 +609,12 @@
             pltpu.VMEM((width, hidden), BF16),
             pltpu.VMEM((width, hidden), BF16),
             pltpu.VMEM((hidden, width), BF16),
-            pltpu.VMEM((batch * capacity, width), BF16),
+            pltpu.VMEM((group * capacity, width), BF16),
             pltpu.VMEM((tokens, width), F32),
             pltpu.VMEM((count, 2, 2, tokens, width), BF16),
             pltpu.VMEM((count, 2, tokens, width), BF16),
-            pltpu.VMEM((1 + count, tokens, half), BF16),
-            pltpu.VMEM((2, 3, count, tokens, half), BF16),
+            pltpu.VMEM((1 + count, tokens, rest), BF16),
+            pltpu.VMEM((2, 3, count, tokens, rest), BF16),
             pltpu.VMEM((2, tokens, width), BF16),
             pltpu.VMEM((tokens, width), BF16),
             pltpu.VMEM((tokens, width), BF16),
@@ -686,8 +754,8 @@
     width = expert_input.shape[1]
     tp_count = lax.axis_size("tp")
     experts = lax.axis_size("ep") * tp_count
-    if tp_count == 4 and experts * tokens * width * 2 <= 8 * 2**20:
-        capacity = max(2, 3 * tokens * top_count // (2 * experts))
+    capacity = max(2, 3 * tokens * top_count // (2 * experts))
+    if tp_count == 4 and capacity % 16 == 0 and experts * tokens * width * 2 <= 8 * 2**20:
         mixer_output, expert_output = exchange(
             terms,
             normalise(expert_input, norm_gain),

time: 177 us -> 152 us (0.86)
  the two profiles are of different devices: /device:TPU:16 before, /device:TPU:0 now
where the time goes in v2:
time: 152 us; the launch traced here: 149 us
  Pallas kernels  127 us (84%)
  other arithmetic  7.79 us (5%)
  local copies, waits for them, and re-layouts  6.43 us (4%)
  starting transfers between devices  4.96 us (3%)
  matrix products  2.24 us (1%)
    pallas_call x1, Pallas kernels, exchange(): pl.pallas_call(lambda *refs: exchange_kernel(capacity, batch, *refs), out...  121 us
    pallas_call x1, Pallas kernels, attend(): pl.pallas_call(attention_kernel, grid=(heads,), out_shape=jax.ShapeDtypeS...  5.59 us
    ppermute x1, starting transfers between devices, passed_along(): return lax.ppermute(block, axis, route)  4.96 us
    unnamed x6, local copies, waits for them, and re-layouts  3.78 us
  transfers between devices with their start and end apart: 1, of which 0 were waited for; matrix products, arithmetic and copies ran while one was open for 4% of the time, Pallas kernels for 0%

profile of v2, /device:TPU:0, one launch (start us, length us, event | category | flops | bytes accessed | tf_op | source)
XLA Modules:
  0.0 148.6 jit_solution(8674012835956634709)
XLA Ops:
  0.6 0.0 copy-start
  0.6 0.0 copy-start.1
  0.7 0.8 reduce
  1.4 0.9 pad_maximum_fusion
  2.4 5.0 %collective-permute-start = (bf16[516,128]{1,0:T(8,128)(2,1)S(1)}, bf16[516,128]{1,0:T(8,128)(2,1)S(1)}, u32[]{:S(2)}, u32[]{:S(2)}) collective-permute-start(bf16[516,128]{1,0:T(8,128)(2,1)S(1)} %get-tuple-element.2), channel_id=1, source_target_pairs={{0,4},{4,8},{8,12},{1,5},{5,9},{9,13},{2,6},{6,10},{10,14},{3,7},{... | collective-permute-start | bytes 396296 | tf_op jit(solution)/shard_map/ppermute | solution.py:16
  7.4 1.2 fusion
  8.6 0.7 fusion.5
  9.3 0.1 convolution_select_fusion
  9.4 2.0 %fusion.2.refs_1_ = bf16[128,2048]{1,0:T(8,128)(2,1)} fusion(bf16[128,2048]{1,0:T(8,128)(2,1)} %param.18, f32[2048]{0:T(1024)} %param.19, f32[128]{0:T(128)S(1)} %add_rsqrt_fusion), kind=kLoop, calls=%fused_computation.6 | loop fusion | flops 1048576 | bytes 1057280 | tf_op jit(solution)/shard_map/convert_element_type | solution.py:651
  11.5 0.7 select_reduce_fusion
  12.2 0.0 copy-done.1
  12.2 0.9 copy.23
  13.1 0.6 select_maximum_fusion.refs_2_
  13.8 0.0 collective-permute-done
  13.8 0.7 fusion.4.kv_ref
  14.5 0.6 reshape.43.bias_ref
  15.1 5.6 %attention.1 = bf16[3,512,64]{2,1,0:T(8,128)(2,1)} custom-call(s32[1]{0:T(128)} %bitcast.place_ref, bf16[3,512,64]{2,1,0:T(8,128)(2,1)} %bitcast.29, bf16[2,1,512,128]{3,2,1,0:T(8,128)(2,1)} %fusion.4.kv_ref, bf16[2,1,1,512]{3,2,1,0:T(2,128)(2,1)} %reshape.43.bias_ref), custom_call_target="tpu_custom_call" | custom-call | flops 4000000000 | bytes 1000000 | tf_op jit(solution)/shard_map/attention/pallas_call | solution.py:102
  20.7 1.1 copy.25
  21.8 0.0 copy-done
  21.8 2.1 %convolution_convert_fusion = bf16[512,2048]{1,0:T(8,128)(2,1)} fusion(bf16[512,192]{0,1:T(8,128)(2,1)S(1)} %bitcast.26, bf16[192,2048]{1,0:T(8,128)(2,1)S(1)} %copy-done), kind=kOutput, calls=%fused_computation | convolution fusion | flops 403701760 | bytes 3080192 | tf_op jit(solution)/shard_map/dot_general | solution.py:129
  23.9 120.9 %exchange.1 = (bf16[128,2048]{1,0:T(8,128)(2,1)}, bf16[128,2048]{1,0:T(8,128)(2,1)}) custom-call(bf16[2,2,128,2048]{3,2,1,0:T(8,128)(2,1)} %bitcast.25, bf16[128,2048]{1,0:T(8,128)(2,1)} %fusion.2.refs_1_, f32[16,8,128]{2,1,0:T(8,128)} %select_maximum_fusion.refs_2_, bf16[2048,256]{1,0:T(8,128)(2,1)} %refs_3_.1, bf16[2048,256]{1,0:T(8,128)(2,1)} %refs_4_.1, ...), custom_call_target="tpu_custom_call" | custom-call | flops 10000000000 | bytes 20000000 | tf_op jit(solution)/shard_map/exchange/pallas_call | solution.py:601
  144.9 1.9 %copy.28 = bf16[128,2048]{1,0:T(8,128)(2,1)} copy(bf16[128,2048]{1,0:T(8,128)(2,1)} %get-tuple-element.6) | data formatting | bytes 1048576
  146.8 1.9 %copy.29 = bf16[128,2048]{1,0:T(8,128)(2,1)} copy(bf16[128,2048]{1,0:T(8,128)(2,1)} %get-tuple-element.7) | data formatting | bytes 1048576
  (2 shorter events, 0.0 us)
Async XLA Ops:
  0.6 21.2 %copy-start = (bf16[192,2048]{1,0:T(8,128)(2,1)S(1)}, bf16[192,2048]{1,0:T(8,128)(2,1)}, u32[]{:S(2)}) copy-start(bf16[192,2048]{1,0:T(8,128)(2,1)} %param.17) | copy-start | bytes 2359300
  0.6 11.6 %copy-start.1 = (bf16[512,192]{0,1:T(8,128)(2,1)S(1)}, bf16[512,192]{0,1:T(8,128)(2,1)}, u32[]{:S(2)}) copy-start(bf16[512,192]{0,1:T(8,128)(2,1)} %param.14) | copy-start | bytes 589828
  2.4 11.4 %collective-permute-start = (bf16[516,128]{1,0:T(8,128)(2,1)S(1)}, bf16[516,128]{1,0:T(8,128)(2,1)S(1)}, u32[]{:S(2)}, u32[]{:S(2)}) collective-permute-start(bf16[516,128]{1,0:T(8,128)(2,1)S(1)} %get-tuple-element.2), channel_id=1, source_target_pairs={{0,4},{4,8},{8,12},{1,5},{5,9},{9,13},{2,6},{6,10},{10,14},{3,7},{... | collective-permute-start | bytes 396296 | tf_op jit(solution)/shard_map/ppermute | solution.py:16

commit v3 on v2

--- a/solution.py
+++ b/solution.py
@@ -178,7 +178,7 @@
     count = lax.axis_size("ep")
     width = normed_ref.shape[1]
     tokens = normed_ref.shape[0]
-    cut = width // 4
+    cut = width // 8
     spans = (slice(0, cut), slice(cut, width))
     pieces = (pl.ds(0, cut), pl.ds(cut, width - cut))
     z = lax.axis_index("ep")
@@ -594,7 +594,7 @@
     count = lax.axis_size("ep")
     group = count * 4
     hidden = routed_parts[0].shape[1]
-    rest = width - width // 4
+    rest = width - width // 8
     batch = 8 if group % 8 == 0 else 4
     dma = pltpu.SemaphoreType.DMA
     vmem = pl.BlockSpec(memory_space=pltpu.VMEM)

time: 152 us -> 148 us (0.974); the launches traced: 149 us -> 148 us
  Pallas kernels: 127 us -> 125 us
where the time goes in v3:
time: 148 us
  Pallas kernels  125 us (84%)
  other arithmetic  7.79 us (5%)
  local copies, waits for them, and re-layouts  6.43 us (4%)
  starting transfers between devices  4.96 us (3%)
  matrix products  2.24 us (2%)
    pallas_call x1, Pallas kernels, exchange(): pl.pallas_call(lambda *refs: exchange_kernel(capacity, batch, *refs), out...  120 us
    pallas_call x1, Pallas kernels, attend(): pl.pallas_call(attention_kernel, grid=(heads,), out_shape=jax.ShapeDtypeS...  5.59 us
    ppermute x1, starting transfers between devices, passed_along(): return lax.ppermute(block, axis, route)  4.96 us
    unnamed x6, local copies, waits for them, and re-layouts  3.78 us
  transfers between devices with their start and end apart: 1, of which 0 were waited for; matrix products, arithmetic and copies ran while one was open for 4% of the time, Pallas kernels for 0%

profile of v3, /device:TPU:0, one launch (start us, length us, event | category | flops | bytes accessed | tf_op | source)
XLA Modules:
  0.0 147.6 jit_solution(12372504665501102360)
XLA Ops:
  0.6 0.0 copy-start
  0.6 0.0 copy-start.1
  0.7 0.8 reduce
  1.4 0.9 pad_maximum_fusion
  2.4 5.0 %collective-permute-start = (bf16[516,128]{1,0:T(8,128)(2,1)S(1)}, bf16[516,128]{1,0:T(8,128)(2,1)S(1)}, u32[]{:S(2)}, u32[]{:S(2)}) collective-permute-start(bf16[516,128]{1,0:T(8,128)(2,1)S(1)} %get-tuple-element.2), channel_id=1, source_target_pairs={{0,4},{4,8},{8,12},{1,5},{5,9},{9,13},{2,6},{6,10},{10,14},{3,7},{... | collective-permute-start | bytes 396296 | tf_op jit(solution)/shard_map/ppermute | solution.py:16
  7.4 1.2 fusion
  8.6 0.7 fusion.5
  9.3 0.1 convolution_select_fusion
  9.4 2.0 %fusion.2.refs_1_ = bf16[128,2048]{1,0:T(8,128)(2,1)} fusion(bf16[128,2048]{1,0:T(8,128)(2,1)} %param.18, f32[2048]{0:T(1024)} %param.19, f32[128]{0:T(128)S(1)} %add_rsqrt_fusion), kind=kLoop, calls=%fused_computation.6 | loop fusion | flops 1048576 | bytes 1057280 | tf_op jit(solution)/shard_map/convert_element_type | solution.py:651
  11.5 0.7 select_reduce_fusion
  12.2 0.0 copy-done.1
  12.2 0.9 copy.23
  13.1 0.6 select_maximum_fusion.refs_2_
  13.8 0.0 collective-permute-done
  13.8 0.7 fusion.4.kv_ref
  14.5 0.6 reshape.43.bias_ref
  15.1 5.6 %attention.1 = bf16[3,512,64]{2,1,0:T(8,128)(2,1)} custom-call(s32[1]{0:T(128)} %bitcast.place_ref, bf16[3,512,64]{2,1,0:T(8,128)(2,1)} %bitcast.29, bf16[2,1,512,128]{3,2,1,0:T(8,128)(2,1)} %fusion.4.kv_ref, bf16[2,1,1,512]{3,2,1,0:T(2,128)(2,1)} %reshape.43.bias_ref), custom_call_target="tpu_custom_call" | custom-call | flops 4000000000 | bytes 1000000 | tf_op jit(solution)/shard_map/attention/pallas_call | solution.py:102
  20.7 1.1 copy.25
  21.8 0.0 copy-done
  21.8 2.1 %convolution_convert_fusion = bf16[512,2048]{1,0:T(8,128)(2,1)} fusion(bf16[512,192]{0,1:T(8,128)(2,1)S(1)} %bitcast.26, bf16[192,2048]{1,0:T(8,128)(2,1)S(1)} %copy-done), kind=kOutput, calls=%fused_computation | convolution fusion | flops 403701760 | bytes 3080192 | tf_op jit(solution)/shard_map/dot_general | solution.py:129
  23.9 119.9 %exchange.1 = (bf16[128,2048]{1,0:T(8,128)(2,1)}, bf16[128,2048]{1,0:T(8,128)(2,1)}) custom-call(bf16[2,2,128,2048]{3,2,1,0:T(8,128)(2,1)} %bitcast.25, bf16[128,2048]{1,0:T(8,128)(2,1)} %fusion.2.refs_1_, f32[16,8,128]{2,1,0:T(8,128)} %select_maximum_fusion.refs_2_, bf16[2048,256]{1,0:T(8,128)(2,1)} %refs_3_.1, bf16[2048,256]{1,0:T(8,128)(2,1)} %refs_4_.1, ...), custom_call_target="tpu_custom_call" | custom-call | flops 10000000000 | bytes 20000000 | tf_op jit(solution)/shard_map/exchange/pallas_call | solution.py:601
  143.8 1.9 %copy.28 = bf16[128,2048]{1,0:T(8,128)(2,1)} copy(bf16[128,2048]{1,0:T(8,128)(2,1)} %get-tuple-element.6) | data formatting | bytes 1048576
  145.7 1.9 %copy.29 = bf16[128,2048]{1,0:T(8,128)(2,1)} copy(bf16[128,2048]{1,0:T(8,128)(2,1)} %get-tuple-element.7) | data formatting | bytes 1048576
  (2 shorter events, 0.0 us)
Async XLA Ops:
  0.6 21.2 %copy-start = (bf16[192,2048]{1,0:T(8,128)(2,1)S(1)}, bf16[192,2048]{1,0:T(8,128)(2,1)}, u32[]{:S(2)}) copy-start(bf16[192,2048]{1,0:T(8,128)(2,1)} %param.17) | copy-start | bytes 2359300
  0.6 11.6 %copy-start.1 = (bf16[512,192]{0,1:T(8,128)(2,1)S(1)}, bf16[512,192]{0,1:T(8,128)(2,1)}, u32[]{:S(2)}) copy-start(bf16[512,192]{0,1:T(8,128)(2,1)} %param.14) | copy-start | bytes 589828
  2.4 11.4 %collective-permute-start = (bf16[516,128]{1,0:T(8,128)(2,1)S(1)}, bf16[516,128]{1,0:T(8,128)(2,1)S(1)}, u32[]{:S(2)}, u32[]{:S(2)}) collective-permute-start(bf16[516,128]{1,0:T(8,128)(2,1)S(1)} %get-tuple-element.2), channel_id=1, source_target_pairs={{0,4},{4,8},{8,12},{1,5},{5,9},{9,13},{2,6},{6,10},{10,14},{3,7},{... | collective-permute-start | bytes 396296 | tf_op jit(solution)/shard_map/ppermute | solution.py:16
